TPU v7x, 32 devices: a whole 2x2x4 slice. The times are simulated.
32 devices in a mesh: ep: 4 (over y, x), tp: 8 (over z, core).
Axes of the slice: x: 2, y: 2, z: 4, core: 2. Of those that a mesh axis runs over, the one named last changes fastest.
Arguments:
- queries: bfloat16 [3072, 2048], P('ep', 'tp'), may hold values from -6 to 6
- keys: bfloat16 [3072, 512], P('ep'), may hold values from -6 to 6
- values: bfloat16 [3072, 512], P('ep'), may hold values from -6 to 6
- query_gain: float32 [128], replicated, may hold values from 1 to 4.5
- key_gain: float32 [128], replicated, may hold values from 1 to 4.5
- out_weight: bfloat16 [2048, 2048], P('tp'), may hold values from -0.75 to 0.75
- tokens_b: bfloat16 [1536, 2048], P('ep'), may hold values from -6 to 6
- norm_gain: float32 [2048], replicated, may hold values from 0.1 to 1.9
- routes: int32 [1536, 2], P('ep'), may hold values from 0 to 15, all different within a row; in each aligned block of 48 rows (0 to 47, 48 to 95, ...) at most 8 rows name the same one
- route_weight: float32 [1536, 2], P('ep'), may hold values from 0.2 to 1
- gate_weight: bfloat16 [16, 2048, 4096], P('ep', None, 'tp'), may hold values from -0.125 to 0.125
- up_weight: bfloat16 [16, 2048, 4096], P('ep', None, 'tp'), may hold values from -0.125 to 0.125
- down_weight: bfloat16 [16, 4096, 2048], P('ep', 'tp'), may hold values from -0.09375 to 0.09375
Outputs:
- mixed_out: bfloat16 [3072, 2048], P(('ep', 'tp'))
- expert_out: bfloat16 [1536, 2048], P(('ep', 'tp'))
Inputs may be any that keep to these rules, and one draw needn't show every extreme that they name: `routes`: A row names 2 different experts. In each aligned block of 48 rows no expert is named more than 8 times, a bound that some block reaches.
All inputs are finite; a program needn't handle non-finite values.
Results may differ from a plain program's by a relative error of at most 0.019.
Values may be sent and summed in bfloat16 or wider, within the bound.
No kernel may reach another device: no remote copies, remote signals or barrier semaphores. Data moves between devices by JAX's collectives and lax.ppermute only.
A program may use at most 128 MiB of HBM per device.

v0:
```python
import jax
import jax.numpy as jnp
from jax import lax
from jax.sharding import PartitionSpec as P

D = 2048
HD = 128
HQ = 16
KVH = 4
EXPERTS = 16
TOPK = 2
GRID_W = 64
CAP = 8
EPS = 1e-06
THETA = 10000.0


def rotate(field, positions):
    n_freq = HD // 4
    row_pos = (positions // GRID_W).astype(jnp.float32)
    col_pos = (positions % GRID_W).astype(jnp.float32)
    inverse = THETA ** (-jnp.arange(n_freq, dtype=jnp.float32) / n_freq)
    angles = jnp.stack([row_pos[:, None] * inverse, col_pos[:, None] * inverse], axis=1)
    cosine = jnp.cos(angles)[:, None]
    sine = jnp.sin(angles)[:, None]
    length, n_heads = (field.shape[0], field.shape[1])
    halves = field.reshape(length, n_heads, 2, 2, n_freq)
    leading = halves[..., 0, :]
    second = halves[..., 1, :]
    turned = jnp.stack(
        [leading * cosine - second * sine, second * cosine + leading * sine], axis=-2
    )
    return turned.reshape(length, n_heads, HD)


def prepare(source, gain_vec, positions, n_heads):
    length = source.shape[0]
    field = source.astype(jnp.float32).reshape(length, n_heads, HD)
    field = field * lax.rsqrt(jnp.mean(field * field, axis=-1, keepdims=True) + EPS) * gain_vec
    return rotate(field, positions).astype(jnp.bfloat16)


def token_mixer(queries, keys, values, query_gain, key_gain, out_weight):
    n_rows = queries.shape[0]
    q_heads = queries.shape[1] // HD
    positions = lax.axis_index("ep") * n_rows + jnp.arange(n_rows, dtype=jnp.int32)
    query_n = prepare(queries, query_gain, positions, q_heads).reshape(n_rows * q_heads, HD)
    kv_index = lax.axis_index("tp") * q_heads // (HQ // KVH)
    own_keys = prepare(
        lax.dynamic_slice_in_dim(keys, kv_index * HD, HD, 1), key_gain, positions, 1
    ).reshape(n_rows, HD)
    own_values = lax.dynamic_slice_in_dim(values, kv_index * HD, HD, 1)
    score_scale = HD ** (-0.5)
    start_state = (
        jnp.full((n_rows * q_heads,), -1e30, jnp.float32),
        jnp.zeros((n_rows * q_heads,), jnp.float32),
        jnp.zeros((n_rows * q_heads, HD), jnp.float32),
    )
    key_piece = lax.all_gather(own_keys, "ep", axis=0, tiled=True)
    value_piece = lax.all_gather(own_values, "ep", axis=0, tiled=True)
    steps_n = key_piece.shape[0] // n_rows

    def one_block(index_b, state):
        running_max, totals, numerator = state
        key_blk = lax.dynamic_slice_in_dim(key_piece, index_b * n_rows, n_rows, 0)
        value_blk = lax.dynamic_slice_in_dim(value_piece, index_b * n_rows, n_rows, 0)
        scores = (
            jnp.einsum("qd,sd->qs", query_n, key_blk, preferred_element_type=jnp.float32)
            * score_scale
        )
        new_max = jnp.maximum(running_max, jnp.max(scores, axis=1))
        shrink = jnp.exp(running_max - new_max)
        weights = jnp.exp(scores - new_max[:, None])
        totals = totals * shrink + jnp.sum(weights, axis=1)
        numerator = numerator * shrink[:, None] + jnp.dot(
            weights.astype(jnp.bfloat16), value_blk, preferred_element_type=jnp.float32
        )
        return (new_max, totals, numerator)

    running_max, totals, numerator = lax.fori_loop(0, steps_n, one_block, start_state)
    attended = (numerator / totals[:, None]).astype(jnp.bfloat16).reshape(n_rows, q_heads * HD)
    return lax.psum_scatter(
        jnp.dot(attended, out_weight, preferred_element_type=jnp.float32).astype(jnp.bfloat16),
        "tp",
        scatter_dimension=0,
        tiled=True,
    )


def expert_half(tokens_b, norm_gain, routes, route_weight, gate_weight, up_weight, down_weight):
    n_tp = lax.axis_size("tp")
    n_ep = lax.axis_size("ep")
    tp_index = lax.axis_index("tp")
    local_rows = tokens_b.shape[0]
    block_rows = local_rows // n_tp
    picks = block_rows * TOPK
    local_experts = gate_weight.shape[0]
    assigned = routes.reshape(n_tp, picks)
    onehot = (assigned[:, :, None] == jnp.arange(EXPERTS, dtype=jnp.int32)[None, None, :]).astype(
        jnp.int32
    )
    slot_rank = jnp.sum((jnp.cumsum(onehot, axis=1) - onehot) * onehot, axis=-1)
    target = assigned * CAP + slot_rank
    target_hot = (
        target[:, :, None] == jnp.arange(EXPERTS * CAP, dtype=jnp.int32)[None, None, :]
    ).astype(jnp.float32)
    token_hot = (
        jnp.arange(picks, dtype=jnp.int32)[:, None] // TOPK
        == jnp.arange(block_rows, dtype=jnp.int32)[None, :]
    ).astype(jnp.float32)
    field = tokens_b.astype(jnp.float32)
    normed = (
        field * lax.rsqrt(jnp.mean(field * field, axis=-1, keepdims=True) + EPS) * norm_gain
    ).astype(jnp.bfloat16)
    dispatch_mat = jnp.einsum(
        "baj,at->bjt", target_hot, token_hot, precision=lax.Precision.HIGHEST
    ).astype(jnp.bfloat16)
    outgoing = jnp.einsum(
        "bjt,btd->bjd",
        dispatch_mat,
        normed.reshape(n_tp, block_rows, D),
        preferred_element_type=jnp.float32,
    )
    outgoing = outgoing.astype(jnp.bfloat16).reshape(n_tp, EXPERTS, CAP, D)
    arrived = lax.all_to_all(outgoing, "ep", split_axis=1, concat_axis=2, tiled=True)
    flat_rows = arrived.reshape(-1, D)
    share_rows = flat_rows.shape[0] // n_tp
    expert_slab_rows = flat_rows.reshape(
        share_rows * lax.axis_size("tp") // share_rows, local_experts, n_ep * CAP, D
    )
    gate_act = jnp.einsum(
        "blmd,ldf->blmf", expert_slab_rows, gate_weight, preferred_element_type=jnp.float32
    )
    up_act = jnp.einsum(
        "blmd,ldf->blmf", expert_slab_rows, up_weight, preferred_element_type=jnp.float32
    )
    hidden = (jax.nn.silu(gate_act) * up_act).astype(jnp.bfloat16)
    result = jnp.einsum("blmf,lfd->blmd", hidden, down_weight, preferred_element_type=jnp.float32)
    summed = lax.psum_scatter(
        result.reshape(-1, D).astype(jnp.bfloat16), "tp", scatter_dimension=0, tiled=True
    )
    returned = lax.all_to_all(
        summed.reshape(local_experts, n_ep, CAP, D), "ep", split_axis=1, concat_axis=0, tiled=True
    )
    returned = returned.reshape(EXPERTS * CAP, D)
    own_target = lax.dynamic_index_in_dim(target_hot, tp_index, 0, keepdims=False)
    shares = (route_weight / jnp.sum(route_weight, axis=-1, keepdims=True)).reshape(n_tp, picks)
    own_shares = lax.dynamic_index_in_dim(shares, tp_index, 0, keepdims=False)
    combine = jnp.einsum(
        "at,aj->tj", token_hot, own_target * own_shares[:, None], precision=lax.Precision.HIGHEST
    )
    return jnp.dot(combine, returned.astype(jnp.float32), precision=lax.Precision.HIGHEST).astype(
        jnp.bfloat16
    )


def on_device(
    queries,
    keys,
    values,
    query_gain,
    key_gain,
    out_weight,
    tokens_b,
    norm_gain,
    routes,
    route_weight,
    gate_weight,
    up_weight,
    down_weight,
):
    mixed_out = token_mixer(queries, keys, values, query_gain, key_gain, out_weight)
    expert_out = expert_half(
        tokens_b, norm_gain, routes, route_weight, gate_weight, up_weight, down_weight
    )
    return (mixed_out, expert_out)


def solution(mesh):
    placed = (
        P("ep", "tp"),
        P("ep", None),
        P("ep", None),
        P(),
        P(),
        P("tp", None),
        P("ep", None),
        P(),
        P("ep", None),
        P("ep", None),
        P("ep", None, "tp"),
        P("ep", None, "tp"),
        P("ep", "tp", None),
    )
    return jax.shard_map(
        on_device,
        mesh=mesh,
        in_specs=placed,
        out_specs=(P(("ep", "tp"), None), P(("ep", "tp"), None)),
        check_vma=False,
    )
```

profile of v0, /device:TPU:0, one launch (start us, length us, event | category | flops | bytes accessed | tf_op | source)
XLA Modules:
  0.0 199.7 jit_solution(16089087401707294677)
XLA Ops:
  7.2 1.9 fusion.24
  9.1 0.8 copy.47
  10.1 1.9 select_reduce_fusion
  12.5 1.8 fusion.26
  14.3 1.3 convert_bitcast_fusion.1
  15.6 2.3 %copy.51 = bf16[8,16,8,2048]{3,2,0,1:T(8,128)(2,1)} copy(bf16[8,16,8,2048]{3,2,1,0:T(8,128)(2,1)S(1)} %convert_bitcast_fusion.1) | data formatting | bytes 8388608 | tf_op jit(solution)/shard_map/reshape | solution.py:124
  17.9 5.3 %all-to-all-start = ((bf16[8,16,8,2048]{3,2,0,1:T(8,128)(2,1)}), bf16[8,16,8,2048]{3,2,0,1:T(8,128)(2,1)}, u32[]{:S(2)}, u32[]{:S(2)}) async-start(bf16[8,16,8,2048]{3,2,0,1:T(8,128)(2,1)} %copy.51), calls=%async_computation.1 | async-start | bytes 8388608 | tf_op jit(solution)/shard_map/all_to_all | solution.py:125
  24.7 47.1 %all-to-all-done = bf16[8,16,8,2048]{3,2,0,1:T(8,128)(2,1)} async-done(((bf16[8,16,8,2048]{3,2,0,1:T(8,128)(2,1)}), bf16[8,16,8,2048]{3,2,0,1:T(8,128)(2,1)}, u32[]{:S(2)}, u32[]{:S(2)}) %all-to-all-start) | async-done | bytes 4194336 | tf_op jit(solution)/shard_map/all_to_all | solution.py:125
  71.8 8.4 %fusion.16 = f32[4,8,32,512]{3,2,1,0:T(8,128)} fusion(bf16[4,2048,512]{2,1,0:T(8,128)(2,1)} %param.25, bf16[8,4,4,8,2048]{4,3,0,2,1:T(8,128)(2,1)} %bitcast.11), kind=kOutput, calls=%fused_computation.22 | convolution fusion | flops 2147483648 | bytes 14680064 | tf_op jit(solution)/shard_map/blmd,ldf->blmf/dot_general | solution.py:131
  80.2 14.2 %convert_bitcast_fusion = bf16[8,4,32,2048]{3,2,0,1:T(8,128)(2,1)} fusion(bf16[4,512,2048]{2,1,0:T(8,128)(2,1)} %param.27, f32[4,8,32,512]{3,2,1,0:T(8,128)} %fusion.16, bf16[4,2048,512]{2,1,0:T(8,128)(2,1)} %param.26, bf16[8,4,4,8,2048]{4,3,0,2,1:T(8,128)(2,1)} %bitcast.11), kind=kOutput, calls=%fused_computation.26 | convolution fusion | flops 4300210176 | bytes 27262976 | tf_op jit(solution)/shard_map/blmf,lfd->blmd/dot_general | solution.py:138
  94.4 4.7 %copy.53 = bf16[8,4,32,2048]{3,2,1,0:T(8,128)(2,1)} copy(bf16[8,4,32,2048]{3,2,0,1:T(8,128)(2,1)} %convert_bitcast_fusion) | data formatting | bytes 8388608 | tf_op jit(solution)/shard_map/convert_element_type | solution.py:140
  99.3 0.9 constant_dynamic-slice_fusion.2
  100.5 2.9 %copy.45 = bf16[768,2,2,2,32]{4,3,2,1,0:T(2,128)(2,1)} copy(bf16[768,2,2,2,32]{0,4,3,2,1:T(8,128)(2,1)S(1)} %pad_maximum_fusion) | data formatting | bytes 786432 | tf_op jit(solution)/shard_map/stack | solution.py:30
  103.4 3.7 %convert_element_type.88 = bf16[1536,128]{1,0:T(8,128)(2,1)S(1)} reshape(bf16[768,2,2,2,32]{4,3,2,1,0:T(2,128)(2,1)} %copy.45) | data formatting | bytes 786432 | tf_op jit(solution)/shard_map/convert_element_type | solution.py:40
  107.1 0.9 constant_dynamic-slice_fusion.1
  109.0 12.7 %all_gather.6 = bf16[3072,128]{0,1:T(8,128)(2,1)S(1)} all-gather(bf16[768,128]{0,1:T(8,128)(2,1)S(1)} %bitcast.98), channel_id=1, replica_groups=mesh['ep'=4,'tp'=8] {'ep'}, dimensions={0}, use_global_device_ids=true | all-gather | bytes 983040 | tf_op jit(solution)/shard_map/all_gather | solution.py:59
  121.7 11.2 %all_gather.7 = bf16[3072,128]{1,0:T(8,128)(2,1)} all-gather(bf16[768,128]{1,0:T(8,128)(2,1)S(1)} %constant_dynamic-slice_fusion.1), channel_id=1, replica_groups=mesh['ep'=4,'tp'=8] {'ep'}, dimensions={0}, use_global_device_ids=true | all-gather | bytes 983040 | tf_op jit(solution)/shard_map/all_gather | solution.py:60
  132.9 15.4 %while.18 = (s32[]{:T(128)}, f32[1536]{0:T(1024)S(1)}, f32[1536]{0:T(1024)S(1)}, f32[1536,128]{1,0:T(8,128)S(1)}, bf16[3072,128]{0,1:T(8,128)(2,1)S(1)}, /*index...) while((s32[]{:T(128)}, f32[1536]{0:T(1024)S(1)}, ...), condition=%wide.region_5.6_spmd.clone, body=%wide.region_2.5_spmd.clone.sunk | while | flops 614014464 | bytes 16613559 | solution.py:80
  132.9 0.8 multiply_reduce_fusion.2
  134.6 2.1 %convolution_add_fusion.2 = f32[1536,128]{1,0:T(8,128)S(1)} fusion(f32[768,1536]{1,0:T(8,128)S(1)} %get-tuple-element.254, f32[1536]{0:T(1024)S(1)} %select_maximum_fusion.2, f32[1536,128]{1,0:T(8,128)S(1)} %get-tuple-element.271, f32[1536]{0:T(1024)S(1)} %get-tuple-element.256, pred[]{:T(512)S(6)} %compare.22, ...), kind=kOutput, calls=%fused_computation.4.clone.1 | convolution fusion | flops 306118656 | bytes 6500357 | tf_op jit(solution)/shard_map/while/body/eval_jaxpr/dot_general | solution.py:75
  136.8 0.8 multiply_reduce_fusion.2
  138.4 2.1 %convolution_add_fusion.2 = f32[1536,128]{1,0:T(8,128)S(1)} fusion(f32[768,1536]{1,0:T(8,128)S(1)} %get-tuple-element.254, f32[1536]{0:T(1024)S(1)} %select_maximum_fusion.2, f32[1536,128]{1,0:T(8,128)S(1)} %get-tuple-element.271, f32[1536]{0:T(1024)S(1)} %get-tuple-element.256, pred[]{:T(512)S(6)} %compare.22, ...), kind=kOutput, calls=%fused_computation.4.clone.1 | convolution fusion | flops 306118656 | bytes 6500357 | tf_op jit(solution)/shard_map/while/body/eval_jaxpr/dot_general | solution.py:75
  140.6 0.8 multiply_reduce_fusion.2
  142.3 2.2 %convolution_add_fusion.2 = f32[1536,128]{1,0:T(8,128)S(1)} fusion(f32[768,1536]{1,0:T(8,128)S(1)} %get-tuple-element.254, f32[1536]{0:T(1024)S(1)} %select_maximum_fusion.2, f32[1536,128]{1,0:T(8,128)S(1)} %get-tuple-element.271, f32[1536]{0:T(1024)S(1)} %get-tuple-element.256, pred[]{:T(512)S(6)} %compare.22, ...), kind=kOutput, calls=%fused_computation.4.clone.1 | convolution fusion | flops 306118656 | bytes 6500357 | tf_op jit(solution)/shard_map/while/body/eval_jaxpr/dot_general | solution.py:75
  144.5 0.8 multiply_reduce_fusion.2
  146.1 2.2 %convolution_add_fusion.2 = f32[1536,128]{1,0:T(8,128)S(1)} fusion(f32[768,1536]{1,0:T(8,128)S(1)} %get-tuple-element.254, f32[1536]{0:T(1024)S(1)} %select_maximum_fusion.2, f32[1536,128]{1,0:T(8,128)S(1)} %get-tuple-element.271, f32[1536]{0:T(1024)S(1)} %get-tuple-element.256, pred[]{:T(512)S(6)} %compare.22, ...), kind=kOutput, calls=%fused_computation.4.clone.1 | convolution fusion | flops 306118656 | bytes 6500357 | tf_op jit(solution)/shard_map/while/body/eval_jaxpr/dot_general | solution.py:75
  148.8 2.7 %convolution_convert_fusion = bf16[768,2048]{1,0:T(8,128)(2,1)} fusion(bf16[768,256]{1,0:T(8,128)(2,1)S(1)} %reshape.431, bf16[256,2048]{1,0:T(8,128)(2,1)S(1)} %copy-done), kind=kOutput, calls=%fused_computation.32 | convolution fusion | flops 806879232 | bytes 4587520 | tf_op jit(solution)/shard_map/dot_general | solution.py:83
  151.7 1.9 copy.54
  153.6 3.5 %all-to-all-start.1 = ((bf16[4,4,8,2048]{3,2,0,1:T(8,128)(2,1)}), bf16[4,4,8,2048]{3,2,0,1:T(8,128)(2,1)S(1)}, u32[]{:S(2)}, u32[]{:S(2)}) async-start(bf16[4,4,8,2048]{3,2,0,1:T(8,128)(2,1)} %copy.54), calls=%async_computation.3 | async-start | bytes 1048576 | tf_op jit(solution)/shard_map/all_to_all | solution.py:142
  157.6 6.0 %all-to-all-done.1 = bf16[4,4,8,2048]{3,2,0,1:T(8,128)(2,1)S(1)} async-done(((bf16[4,4,8,2048]{3,2,0,1:T(8,128)(2,1)}), bf16[4,4,8,2048]{3,2,0,1:T(8,128)(2,1)S(1)}, u32[]{:S(2)}, u32[]{:S(2)}) %all-to-all-start.1) | async-done | bytes 524320 | tf_op jit(solution)/shard_map/all_to_all | solution.py:142
  163.6 1.0 convolution_convert_fusion.1
  164.6 28.2 %reduce-scatter.3.cloned.1.call-done = bf16[96,2048]{1,0:T(8,128)(2,1)} async-done(((bf16[768,2048]{1,0:T(8,128)(2,1)}), bf16[96,2048]{1,0:T(8,128)(2,1)}) %reduce-scatter.3.cloned.1.call-update) | async-done | bytes 393232 | tf_op jit(solution)/shard_map/reduce_scatter | solution.py:82
  (67 shorter events, 7.8 us)
Async XLA Ops:
  7.2 141.6 %copy-start = (bf16[256,2048]{1,0:T(8,128)(2,1)S(1)}, bf16[256,2048]{1,0:T(8,128)(2,1)}, u32[]{:S(2)}) copy-start(bf16[256,2048]{1,0:T(8,128)(2,1)} %param.20) | copy-start | bytes 3145732
  17.9 5.3 %copy-start.3 = (f32[128]{0:T(128)S(1)}, f32[128]{0:T(128)}, u32[]{:S(2)}) copy-start(f32[128]{0:T(128)} %param.18) | copy-start | bytes 1540
  17.9 5.4 %copy-start.1 = (bf16[768,256]{1,0:T(8,128)(2,1)S(1)}, bf16[768,256]{1,0:T(8,128)(2,1)}, u32[]{:S(2)}) copy-start(bf16[768,256]{1,0:T(8,128)(2,1)} %param.15) | copy-start | bytes 1179652
  17.9 53.9 %all-to-all-start = ((bf16[8,16,8,2048]{3,2,0,1:T(8,128)(2,1)}), bf16[8,16,8,2048]{3,2,0,1:T(8,128)(2,1)}, u32[]{:S(2)}, u32[]{:S(2)}) async-start(bf16[8,16,8,2048]{3,2,0,1:T(8,128)(2,1)} %copy.51), calls=%async_computation.1 | async-start | bytes 8388608 | tf_op jit(solution)/shard_map/all_to_all | solution.py:125
  23.2 128.5 %reduce-scatter.5.cloned.1.call-start = ((), (), s32[]{:S(2)}) async-start(), calls=%async_computation.5 | async-start | bytes 4718592 | tf_op jit(solution)/shard_map/reduce_scatter | solution.py:139
  99.1 9.0 %copy-start.4 = (f32[128]{0:T(128)S(1)}, f32[128]{0:T(128)}, u32[]{:S(2)}) copy-start(f32[128]{0:T(128)} %param.19) | copy-start | bytes 1540
  99.1 93.7 %reduce-scatter.3.cloned.1.call-start = ((), (), s32[]{:S(2)}) async-start(), calls=%async_computation.4 | async-start | bytes 3538944 | tf_op jit(solution)/shard_map/reduce_scatter | solution.py:82
  148.7 2.7 %copy-start.2 = (f32[384,2]{0,1:T(2,128)S(1)}, f32[384,2]{0,1:T(2,128)}, u32[]{:S(2)}) copy-start(f32[384,2]{0,1:T(2,128)} %param.24) | copy-start | bytes 9220
  153.6 10.0 %all-to-all-start.1 = ((bf16[4,4,8,2048]{3,2,0,1:T(8,128)(2,1)}), bf16[4,4,8,2048]{3,2,0,1:T(8,128)(2,1)S(1)}, u32[]{:S(2)}, u32[]{:S(2)}) async-start(bf16[4,4,8,2048]{3,2,0,1:T(8,128)(2,1)} %copy.54), calls=%async_computation.3 | async-start | bytes 1048576 | tf_op jit(solution)/shard_map/all_to_all | solution.py:142
Sparse Core Ops, SparseCore 0:
  99.2 50.3 reduce-scatter.4
  152.6 40.2 reduce-scatter.2
where the time goes:
time: 200 us
  waiting for transfers between devices  81.4 us (41%)
  matrix products  40 us (20%)
  blocking collectives  23.9 us (12%)
  local copies, waits for them, and re-layouts  19.3 us (10%)
  between operations  14.3 us (7%)
  other arithmetic  11.5 us (6%)
  starting transfers between devices  9.02 us (5%)
    all_to_all x1, waiting for transfers between devices, expert_half(): lax.all_to_all(outgoing, 'ep', split_axis=1, concat_axis=2, tiled=True)  47.1 us
    reduce_scatter x1, waiting for transfers between devices, token_mixer(): lax.psum_scatter(jnp.dot(attended, out_weight, preferred_element_type=jnp...  28.2 us
    dot_general x1, matrix products, expert_half(): jnp.einsum('blmf,lfd->blmd', hidden, down_weight, preferred_element_type=...  14.2 us
    all_gather x1, blocking collectives, token_mixer(): key_piece = lax.all_gather(own_keys, 'ep', axis=0, tiled=True)  12.7 us
    all_gather x1, blocking collectives, token_mixer(): value_piece = lax.all_gather(own_values, 'ep', axis=0, tiled=True)  11.2 us
    dot_general x4, matrix products, one_block(): jnp.dot(weights.astype(jnp.bfloat16), value_blk, preferred_element_type=j...  8.6 us
    dot_general x1, matrix products, expert_half(): jnp.einsum('blmd,ldf->blmf', expert_slab_rows, gate_weight, preferred_ele...  8.38 us
    all_to_all x1, waiting for transfers between devices, expert_half(): lax.all_to_all(summed.reshape(local_experts, n_ep, CAP, D), 'ep', split_a...  6.01 us
  transfers between devices with their start and end apart: 4, of which 3 were waited for; matrix products, arithmetic and copies ran while one was open for 16% of the time, Pallas kernels for 0%

commit v1 on v0

--- a/solution.py
+++ b/solution.py
@@ -56,8 +56,11 @@
         jnp.zeros((n_rows * q_heads,), jnp.float32),
         jnp.zeros((n_rows * q_heads, HD), jnp.float32),
     )
-    key_piece = lax.all_gather(own_keys, "ep", axis=0, tiled=True)
-    value_piece = lax.all_gather(own_values, "ep", axis=0, tiled=True)
+    key_piece, value_piece = jnp.split(
+        lax.all_gather(jnp.concatenate([own_keys, own_values], axis=1), "ep", axis=0, tiled=True),
+        [own_keys.shape[1]],
+        axis=1,
+    )
     steps_n = key_piece.shape[0] // n_rows
 
     def one_block(index_b, state):

time: 200 us -> 213 us (1.065)
  waiting for transfers between devices: 81.4 us -> 113 us
  blocking collectives: 23.9 us -> 0 us
    all_gather x2 -> x0, blocking collectives: 23.9 us -> none  [the longest x1 12.7 us: token_mixer(): key_piece = lax.all_gather(own_keys, 'ep', axis=0, tiled=True)]
    reduce_scatter x1, waiting for transfers between devices: 0.02 us -> 21.3 us  [expert_half(): lax.psum_scatter(result.reshape(-1, D).astype(jnp.bfloat16), 'tp', scatte...]
    all_to_all x1, waiting for transfers between devices: 47.1 us -> 57.4 us  [expert_half(): lax.all_to_all(outgoing, 'ep', split_axis=1, concat_axis=2, tiled=True)]
    dot_general x4, matrix products: 8.6 us -> 4.89 us  [one_block(): jnp.dot(weights.astype(jnp.bfloat16), value_blk, preferred_element_type=j...]
    dot_general x4, matrix products: 3.31 us -> 6.99 us  [one_block(): jnp.einsum('qd,sd->qs', query_n, key_blk, preferred_element_type=jnp.floa...]
    split x0 -> x1, local copies, waits for them, and re-layouts: none -> 2.35 us  [token_mixer(): jnp.split(lax.all_gather(jnp.concatenate([own_keys, own_values], axis=1),...]
  transfers between devices with their start and end apart: 4 -> 5, of which waited for: 3 -> 4; matrix products, arithmetic and copies ran while one was open for 16% -> 30% of each run, Pallas kernels for 0% -> 0%
where the time goes in v1:
time: 213 us; the launch traced here: 212 us
  waiting for transfers between devices  113 us (53%)
  matrix products  40 us (19%)
  local copies, waits for them, and re-layouts  21 us (10%)
  between operations  15.8 us (7%)
  other arithmetic  12.3 us (6%)
  starting transfers between devices  9.46 us (4%)
    all_to_all x1, waiting for transfers between devices, expert_half(): lax.all_to_all(outgoing, 'ep', split_axis=1, concat_axis=2, tiled=True)  57.4 us
    reduce_scatter x1, waiting for transfers between devices, token_mixer(): lax.psum_scatter(jnp.dot(attended, out_weight, preferred_element_type=jnp...  28.5 us
    reduce_scatter x1, waiting for transfers between devices, expert_half(): lax.psum_scatter(result.reshape(-1, D).astype(jnp.bfloat16), 'tp', scatte...  21.3 us
    dot_general x1, matrix products, expert_half(): jnp.einsum('blmf,lfd->blmd', hidden, down_weight, preferred_element_type=...  14.2 us
    dot_general x1, matrix products, expert_half(): jnp.einsum('blmd,ldf->blmf', expert_slab_rows, gate_weight, preferred_ele...  8.38 us
    dot_general x4, matrix products, one_block(): jnp.einsum('qd,sd->qs', query_n, key_blk, preferred_element_type=jnp.floa...  6.99 us
    all_to_all x1, waiting for transfers between devices, expert_half(): lax.all_to_all(summed.reshape(local_experts, n_ep, CAP, D), 'ep', split_a...  6.05 us
    all_to_all x1, starting transfers between devices, expert_half(): lax.all_to_all(outgoing, 'ep', split_axis=1, concat_axis=2, tiled=True)  5.32 us
  transfers between devices with their start and end apart: 5, of which 4 were waited for; matrix products, arithmetic and copies ran while one was open for 30% of the time, Pallas kernels for 0%

profile of v1, /device:TPU:0, one launch (start us, length us, event | category | flops | bytes accessed | tf_op | source)
XLA Modules:
  0.0 212.0 jit_solution(1187848143734451453)
XLA Ops:
  8.0 1.9 fusion.24
  9.9 0.8 copy.53
  11.0 1.9 select_reduce_fusion
  13.3 1.8 fusion.26
  15.1 1.3 convert_bitcast_fusion.1
  16.4 2.3 %copy.57 = bf16[8,16,8,2048]{3,2,0,1:T(8,128)(2,1)} copy(bf16[8,16,8,2048]{3,2,1,0:T(8,128)(2,1)S(1)} %convert_bitcast_fusion.1) | data formatting | bytes 8388608 | tf_op jit(solution)/shard_map/reshape | solution.py:127
  18.7 5.3 %all-to-all-start = ((bf16[8,16,8,2048]{3,2,0,1:T(8,128)(2,1)}), bf16[8,16,8,2048]{3,2,0,1:T(8,128)(2,1)}, u32[]{:S(2)}, u32[]{:S(2)}) async-start(bf16[8,16,8,2048]{3,2,0,1:T(8,128)(2,1)} %copy.57), calls=%async_computation.1 | async-start | bytes 8388608 | tf_op jit(solution)/shard_map/all_to_all | solution.py:128
  24.0 1.1 constant_dynamic-slice_fusion.1
  27.9 57.4 %all-to-all-done = bf16[8,16,8,2048]{3,2,0,1:T(8,128)(2,1)} async-done(((bf16[8,16,8,2048]{3,2,0,1:T(8,128)(2,1)}), bf16[8,16,8,2048]{3,2,0,1:T(8,128)(2,1)}, u32[]{:S(2)}, u32[]{:S(2)}) %all-to-all-start) | async-done | bytes 4194336 | tf_op jit(solution)/shard_map/all_to_all | solution.py:128
  85.3 8.4 %fusion.16 = f32[4,8,32,512]{3,2,1,0:T(8,128)} fusion(bf16[4,2048,512]{2,1,0:T(8,128)(2,1)} %param.25, bf16[8,4,4,8,2048]{4,3,0,2,1:T(8,128)(2,1)} %bitcast.11), kind=kOutput, calls=%fused_computation.22 | convolution fusion | flops 2147483648 | bytes 14680064 | tf_op jit(solution)/shard_map/blmd,ldf->blmf/dot_general | solution.py:134
  93.7 14.2 %convert_bitcast_fusion = bf16[8,4,32,2048]{3,2,0,1:T(8,128)(2,1)} fusion(bf16[4,512,2048]{2,1,0:T(8,128)(2,1)} %param.27, f32[4,8,32,512]{3,2,1,0:T(8,128)} %fusion.16, bf16[4,2048,512]{2,1,0:T(8,128)(2,1)} %param.26, bf16[8,4,4,8,2048]{4,3,0,2,1:T(8,128)(2,1)} %bitcast.11), kind=kOutput, calls=%fused_computation.26 | convolution fusion | flops 4300210176 | bytes 27262976 | tf_op jit(solution)/shard_map/blmf,lfd->blmd/dot_general | solution.py:141
  107.9 4.7 %copy.59 = bf16[8,4,32,2048]{3,2,1,0:T(8,128)(2,1)} copy(bf16[8,4,32,2048]{3,2,0,1:T(8,128)(2,1)} %convert_bitcast_fusion) | data formatting | bytes 8388608 | tf_op jit(solution)/shard_map/convert_element_type | solution.py:143
  114.0 2.9 %copy.50 = bf16[768,2,2,2,32]{4,3,2,1,0:T(2,128)(2,1)} copy(bf16[768,2,2,2,32]{0,4,3,2,1:T(8,128)(2,1)S(1)} %pad_maximum_fusion.1) | data formatting | bytes 786432 | tf_op jit(solution)/shard_map/stack | solution.py:30
  116.9 3.7 %convert_element_type.88 = bf16[1536,128]{1,0:T(8,128)(2,1)S(1)} reshape(bf16[768,2,2,2,32]{4,3,2,1,0:T(2,128)(2,1)} %copy.50) | data formatting | bytes 786432 | tf_op jit(solution)/shard_map/convert_element_type | solution.py:40
  120.6 2.4 %fusion.71 = (bf16[3072,128]{0,1:T(8,128)(2,1)S(1)}, bf16[3072,128]{0,1:T(8,128)(2,1)}) fusion(bf16[3072,256]{0,1:T(8,128)(2,1)} %all-gather.2.cloned.1.call-done), kind=kLoop, calls=%fused_computation.117 | loop fusion | bytes 3145728 | tf_op jit(solution)/shard_map/split | solution.py:59
  123.0 15.4 %while.18 = (s32[]{:T(128)}, f32[1536]{0:T(1024)S(1)}, f32[1536]{0:T(1024)S(1)}, f32[1536,128]{1,0:T(8,128)S(1)}, bf16[3072,128]{0,1:T(8,128)(2,1)}, /*index=5*/...) while((s32[]{:T(128)}, f32[1536]{0:T(1024)S(1)}, ...), condition=%wide.region_5.6_spmd.clone, body=%wide.region_2.5_spmd.clone.sunk | while | flops 614014464 | bytes 16617655 | solution.py:83
  123.0 1.7 multiply_reduce_fusion.2
  124.7 0.8 fusion.87
  125.5 1.2 convolution_add_fusion.2
  126.8 1.7 multiply_reduce_fusion.2
  129.4 1.2 convolution_add_fusion.2
  130.7 1.8 multiply_reduce_fusion.2
  133.2 1.2 convolution_add_fusion.2
  134.5 1.8 multiply_reduce_fusion.2
  137.1 1.2 convolution_add_fusion.2
  138.8 2.7 %convolution_convert_fusion = bf16[768,2048]{1,0:T(8,128)(2,1)} fusion(bf16[768,256]{1,0:T(8,128)(2,1)S(1)} %reshape.431, bf16[256,2048]{1,0:T(8,128)(2,1)S(1)} %copy-done), kind=kOutput, calls=%fused_computation.32 | convolution fusion | flops 806879232 | bytes 4587520 | tf_op jit(solution)/shard_map/dot_general | solution.py:86
  141.7 21.3 %reduce-scatter.5.cloned.1.call-done = bf16[128,2048]{1,0:T(8,128)(2,1)} async-done(((bf16[1024,2048]{1,0:T(8,128)(2,1)}), bf16[128,2048]{1,0:T(8,128)(2,1)}) %reduce-scatter.5.cloned.1.call-update) | async-done | bytes 524304 | tf_op jit(solution)/shard_map/reduce_scatter | solution.py:142
  163.0 1.9 copy.60
  164.8 3.6 %all-to-all-start.1 = ((bf16[4,4,8,2048]{3,2,0,1:T(8,128)(2,1)}), bf16[4,4,8,2048]{3,2,0,1:T(8,128)(2,1)S(1)}, u32[]{:S(2)}, u32[]{:S(2)}) async-start(bf16[4,4,8,2048]{3,2,0,1:T(8,128)(2,1)} %copy.60), calls=%async_computation.3 | async-start | bytes 1048576 | tf_op jit(solution)/shard_map/all_to_all | solution.py:145
  169.0 6.0 %all-to-all-done.1 = bf16[4,4,8,2048]{3,2,0,1:T(8,128)(2,1)S(1)} async-done(((bf16[4,4,8,2048]{3,2,0,1:T(8,128)(2,1)}), bf16[4,4,8,2048]{3,2,0,1:T(8,128)(2,1)S(1)}, u32[]{:S(2)}, u32[]{:S(2)}) %all-to-all-start.1) | async-done | bytes 524320 | tf_op jit(solution)/shard_map/all_to_all | solution.py:145
  175.1 1.0 convolution_convert_fusion.1
  176.1 28.5 %reduce-scatter.3.cloned.1.call-done = bf16[96,2048]{1,0:T(8,128)(2,1)} async-done(((bf16[768,2048]{1,0:T(8,128)(2,1)}), bf16[96,2048]{1,0:T(8,128)(2,1)}) %reduce-scatter.3.cloned.1.call-update) | async-done | bytes 393232 | tf_op jit(solution)/shard_map/reduce_scatter | solution.py:85
  (70 shorter events, 8.2 us)
Async XLA Ops:
  8.0 130.8 %copy-start = (bf16[256,2048]{1,0:T(8,128)(2,1)S(1)}, bf16[256,2048]{1,0:T(8,128)(2,1)}, u32[]{:S(2)}) copy-start(bf16[256,2048]{1,0:T(8,128)(2,1)} %param.20) | copy-start | bytes 3145732
  18.7 6.9 %copy-start.4 = (f32[128]{0:T(128)S(1)}, f32[128]{0:T(128)}, u32[]{:S(2)}) copy-start(f32[128]{0:T(128)} %param.19) | copy-start | bytes 1540
  18.7 66.6 %all-to-all-start = ((bf16[8,16,8,2048]{3,2,0,1:T(8,128)(2,1)}), bf16[8,16,8,2048]{3,2,0,1:T(8,128)(2,1)}, u32[]{:S(2)}, u32[]{:S(2)}) async-start(bf16[8,16,8,2048]{3,2,0,1:T(8,128)(2,1)} %copy.57), calls=%async_computation.1 | async-start | bytes 8388608 | tf_op jit(solution)/shard_map/all_to_all | solution.py:128
  24.0 3.5 %copy-start.1 = (bf16[768,256]{1,0:T(8,128)(2,1)S(1)}, bf16[768,256]{1,0:T(8,128)(2,1)}, u32[]{:S(2)}) copy-start(bf16[768,256]{1,0:T(8,128)(2,1)} %param.15) | copy-start | bytes 1179652
  24.0 96.6 %all-gather.2.cloned.1.call-start = ((), (), s32[]{:S(2)}) async-start(), calls=%async_computation.4 | async-start | bytes 1966080 | tf_op jit(solution)/shard_map/all_gather | solution.py:60
  27.3 135.7 %reduce-scatter.5.cloned.1.call-start = ((), (), s32[]{:S(2)}) async-start(), calls=%async_computation.6 | async-start | bytes 4718592 | tf_op jit(solution)/shard_map/reduce_scatter | solution.py:142
  112.6 1.0 copy-start.3
  112.6 92.0 %reduce-scatter.3.cloned.1.call-start = ((), (), s32[]{:S(2)}) async-start(), calls=%async_computation.5 | async-start | bytes 3538944 | tf_op jit(solution)/shard_map/reduce_scatter | solution.py:85
  138.8 2.7 %copy-start.2 = (f32[384,2]{0,1:T(2,128)S(1)}, f32[384,2]{0,1:T(2,128)}, u32[]{:S(2)}) copy-start(f32[384,2]{0,1:T(2,128)} %param.24) | copy-start | bytes 9220
  164.8 10.2 %all-to-all-start.1 = ((bf16[4,4,8,2048]{3,2,0,1:T(8,128)(2,1)}), bf16[4,4,8,2048]{3,2,0,1:T(8,128)(2,1)S(1)}, u32[]{:S(2)}, u32[]{:S(2)}) async-start(bf16[4,4,8,2048]{3,2,0,1:T(8,128)(2,1)} %copy.60), calls=%async_computation.3 | async-start | bytes 1048576 | tf_op jit(solution)/shard_map/all_to_all | solution.py:145
Sparse Core Ops, SparseCore 0:
  27.4 56.3 all-gather.1
Sparse Core Ops, SparseCore 1:
  112.7 50.2 reduce-scatter.4
  165.7 38.8 reduce-scatter.2
